TPU v7x, 32 devices: a whole 2x2x4 slice. The times are simulated.
32 devices in a mesh: rep: 2 (over x), fs: 8 (over z, y), tp: 2 (over core).
Axes of the slice: x: 2, y: 2, z: 4, core: 2. Of those that a mesh axis runs over, the one named last changes fastest.
Arguments:
- tokens: bfloat16 [10240, 2048], P(('rep', 'fs'), 'tp'), may hold values from -6 to 6
- norm_first: float32 [2048], replicated, may hold values from 0.1 to 1.9
- norm_mix: float32 [2048], replicated, may hold values from 0.1 to 1.9
- norm_second: float32 [2048], replicated, may hold values from 0.1 to 1.9
- gate_weight: float32 [2048, 2816], P('fs', 'tp'), may hold values from -0.125 to 0.125
- up_weight: float32 [2048, 2816], P('fs', 'tp'), may hold values from -0.125 to 0.125
- down_weight: float32 [2816, 2048], P('tp', 'fs'), may hold values from -0.109375 to 0.109375
- gate_scale: float32 [2816], P('tp'), may hold values from 0.3 to 3
- up_scale: float32 [2816], P('tp'), may hold values from 0.3 to 3
- down_scale: float32 [2048], P('fs'), may hold values from 0.3 to 3
- u_weight: float32 [2048, 1024], P('fs', 'tp'), may hold values from -0.125 to 0.125
- v_weight: float32 [2048, 1024], P('fs', 'tp'), may hold values from -0.125 to 0.125
- u_scale: float32 [1024], P('tp'), may hold values from 0.3 to 3
- v_scale: float32 [1024], P('tp'), may hold values from 0.15 to 6
- ln_gain: float32 [1024], P('tp'), may hold values from 0.1 to 1.9
- ln_bias: float32 [1024], P('tp'), may hold values from -3 to 3
- spatial_weight: bfloat16 [8, 128, 128], P('tp'), may hold values from -0.25 to 0.25
- spatial_bias: float32 [8, 128], P('tp'), may hold values from 0.1 to 1.9
- out_weight: float32 [1024, 2048], P('tp', 'fs'), may hold values from -0.1875 to 0.1875
- out_scale: float32 [2048], P('fs'), may hold values from 0.3 to 3
Outputs:
- layer_out: bfloat16 [10240, 2048], P(('rep', 'fs'), 'tp')
All inputs are finite; a program needn't handle non-finite values.
Results may differ from a plain program's by a relative error of at most 0.019.
Values may be sent and summed in bfloat16 or wider, within the bound.
No kernel may reach another device: no remote copies, remote signals or barrier semaphores. Data moves between devices by JAX's collectives and lax.ppermute only.
A program may use at most 128 MiB of HBM per device.

v0:
```python
import jax
import jax.numpy as jnp
from jax import lax
from jax.sharding import PartitionSpec as P

BW = 1024
SPAN = 128
EPS = 1e-06


def add_pair(left, pieces):
    return (
        jnp.dot(left, pieces[0], preferred_element_type=jnp.float32),
        jnp.dot(left, pieces[1], preferred_element_type=jnp.float32),
    )


def on_device(
    tokens,
    norm_first,
    norm_mix,
    norm_second,
    gate_weight,
    up_weight,
    down_weight,
    gate_scale,
    up_scale,
    down_scale,
    u_weight,
    v_weight,
    u_scale,
    v_scale,
    ln_gain,
    ln_bias,
    spatial_weight,
    spatial_bias,
    out_weight,
    out_scale,
):
    wide_scales = (
        lax.all_gather(down_scale, "fs", axis=0, tiled=True),
        lax.all_gather(out_scale, "fs", axis=0, tiled=True),
    )
    gate_low = gate_weight.astype(jnp.bfloat16)
    up_low = up_weight.astype(jnp.bfloat16)
    down_low = down_weight.astype(jnp.bfloat16)
    count = tokens.shape[0]

    def full_norm(rows, gain):
        whole = lax.all_gather(rows, "tp", axis=1, tiled=True)
        values = whole.astype(jnp.float32)
        factor = lax.rsqrt(jnp.mean(values * values, axis=1, keepdims=True) + EPS)
        return (values * factor * gain).astype(jnp.bfloat16)

    def spread_sum(term):
        return lax.psum_scatter(
            term.astype(jnp.bfloat16), "tp", scatter_dimension=1, tiled=True
        ).astype(jnp.float32)

    gate_all, up_all = (
        lax.all_gather(gate_low, "fs", axis=0, tiled=True),
        lax.all_gather(up_low, "fs", axis=0, tiled=True),
    )

    def hidden_units(normed):
        gate = jnp.dot(normed, gate_all, preferred_element_type=jnp.float32) * gate_scale
        up_part = jnp.dot(normed, up_all, preferred_element_type=jnp.float32) * up_scale
        return (jax.nn.silu(gate) * up_part).astype(jnp.bfloat16)

    first_hidden = hidden_units(full_norm(tokens, norm_first))
    down_all = lax.all_gather(down_low, "fs", axis=1, tiled=True)
    first_term = (
        jnp.dot(first_hidden, down_all, preferred_element_type=jnp.float32) * wide_scales[0]
    )
    first = spread_sum(first_term)
    middle = (tokens.astype(jnp.float32) + 0.5 * first).astype(jnp.bfloat16)
    mix_normed = full_norm(middle, norm_mix)
    u_low = u_weight.astype(jnp.bfloat16)
    v_low = v_weight.astype(jnp.bfloat16)
    u_acc, v_acc = add_pair(
        mix_normed,
        (
            lax.all_gather(u_low, "fs", axis=0, tiled=True),
            lax.all_gather(v_low, "fs", axis=0, tiled=True),
        ),
    )
    u_pre = u_acc * u_scale
    v_act = jax.nn.gelu(v_acc * v_scale, approximate=True)
    totals = lax.psum((jnp.sum(v_act, axis=1), jnp.sum(v_act * v_act, axis=1)), "tp")
    v_mean = (totals[0] / BW)[:, None]
    v_var = (totals[1] / BW)[:, None] - v_mean * v_mean
    v_normed = ((v_act - v_mean) * lax.rsqrt(v_var + EPS) * ln_gain + ln_bias).astype(jnp.bfloat16)
    local_groups = spatial_weight.shape[0]
    channels = v_act.shape[1] // local_groups
    blocks = v_normed.reshape(count // SPAN, SPAN, local_groups, channels)
    lower = jnp.tril(jnp.ones((SPAN, SPAN), jnp.bool_))
    masked = jnp.where(lower[None], spatial_weight, jnp.zeros_like(spatial_weight))
    spatial = jnp.einsum("gts,nsgc->ntgc", masked, blocks, preferred_element_type=jnp.float32)
    spatial = spatial + spatial_bias.T[None, :, :, None]
    mixed = (jax.nn.gelu(u_pre, approximate=True) * spatial.reshape(count, v_act.shape[1])).astype(
        jnp.bfloat16
    )
    out_low = out_weight.astype(jnp.bfloat16)
    mix_term = (
        jnp.dot(
            mixed,
            lax.all_gather(out_low, "fs", axis=1, tiled=True),
            preferred_element_type=jnp.float32,
        )
        * wide_scales[1]
    )
    second = (middle.astype(jnp.float32) + spread_sum(mix_term)).astype(jnp.bfloat16)
    second_hidden = hidden_units(full_norm(second, norm_second))
    last = spread_sum(
        jnp.dot(second_hidden, down_all, preferred_element_type=jnp.float32) * wide_scales[0]
    )
    return (second.astype(jnp.float32) + 0.5 * last).astype(jnp.bfloat16)


def solution(mesh):
    placed = (
        P(("rep", "fs"), "tp"),
        P(),
        P(),
        P(),
        P("fs", "tp"),
        P("fs", "tp"),
        P("tp", "fs"),
        P("tp"),
        P("tp"),
        P("fs"),
        P("fs", "tp"),
        P("fs", "tp"),
        P("tp"),
        P("tp"),
        P("tp"),
        P("tp"),
        P("tp", None, None),
        P("tp", None),
        P("tp", "fs"),
        P("fs"),
    )
    return jax.shard_map(
        on_device, mesh=mesh, in_specs=placed, out_specs=P(("rep", "fs"), "tp"), check_vma=False
    )
```

profile of v0, /device:TPU:0, one launch (start us, length us, event | category | flops | bytes accessed | tf_op | source)
XLA Modules:
  0.0 577.7 jit_solution(11312762153509955955)
XLA Ops:
  7.3 2.4 convert_element_type.87
  9.8 0.9 convert_element_type.88
  10.9 0.9 convert_element_type.90
  11.9 22.3 %all-gather = f32[8,1,256]{2,1,0:T(1,128)S(1)} all-gather(f32[1,1,256]{2,1,0:T(1,128)S(1)} %bitcast.34), channel_id=1, replica_groups=mesh['rep'=2,'fs'=8,'tp'=2] {'fs'}, dimensions={0}, use_global_device_ids=true | all-gather | bytes 9216 | tf_op jit(solution)/shard_map/all_gather | solution.py:41
  34.2 2.6 fusion
  36.9 81.8 %all-gather.14.cloned.1.call-done = bf16[2048,1408]{1,0:T(8,128)(2,1)} async-done(((bf16[256,1408]{1,0:T(8,128)(2,1)}), bf16[2048,1408]{1,0:T(8,128)(2,1)}) %all-gather.14.cloned.1.call-update) | async-done | bytes 5767184 | tf_op jit(solution)/shard_map/all_gather | solution.py:61
  118.7 8.7 %convolution_multiply_fusion.3 = f32[640,1408]{1,0:T(8,128)} fusion(bf16[2048,1408]{1,0:T(8,128)(2,1)} %all-gather.14.cloned.1.call-done, f32[1408]{0:T(1024)S(1)} %copy-done.19, bf16[640,2048]{1,0:T(8,128)(2,1)S(1)} %copy-done.4, f32[2048]{0:T(1024)S(1)} %copy-done.17, f32[640]{0:T(1024)S(1)} %add_rsqrt_fusion.3), kind=kOutput, calls=%fused_computation.23 | convolution fusion | flops 3697131520 | bytes 12009472 | tf_op jit(solution)/shard_map/dot_general | solution.py:66
  127.4 84.0 %all-gather.16.cloned.1.call-done = bf16[2048,1408]{1,0:T(8,128)(2,1)} async-done(((bf16[256,1408]{1,0:T(8,128)(2,1)}), bf16[2048,1408]{1,0:T(8,128)(2,1)}) %all-gather.16.cloned.1.call-update) | async-done | bytes 5767184 | tf_op jit(solution)/shard_map/all_gather | solution.py:62
  211.4 93.2 %all-gather.18.cloned.1.call-done = bf16[1408,2048]{1,0:T(8,128)(2,1)} async-done(((bf16[1408,256]{1,0:T(8,128)(2,1)}), bf16[1408,2048]{1,0:T(8,128)(2,1)}) %all-gather.18.cloned.1.call-update) | async-done | bytes 5767184 | tf_op jit(solution)/shard_map/all_gather | solution.py:71
  304.6 15.4 %multiply_convert_fusion.2 = bf16[640,2048]{1,0:T(8,128)(2,1)} fusion(bf16[1408,2048]{1,0:T(8,128)(2,1)} %all-gather.18.cloned.1.call-done, f32[2048]{0:T(1024)S(1)} %bitcast.30, bf16[2048,1408]{1,0:T(8,128)(2,1)} %all-gather.16.cloned.1.call-done, f32[640,1408]{1,0:T(8,128)} %convolution_multiply_fusion.3, f32[1408]{0:T(1024)S(1)} %copy-done.20, ...), kind=kOutput, calls=%fused_computation.17 | convolution fusion | flops 7396147200 | bytes 20406272 | tf_op jit(solution)/shard_map/dot_general | solution.py:73
  320.1 8.5 %reduce-scatter.4.cloned.1.call-done = bf16[640,1024]{1,0:T(8,128)(2,1)} async-done(((bf16[640,2048]{1,0:T(8,128)(2,1)}), bf16[640,1024]{1,0:T(8,128)(2,1)}) %reduce-scatter.4.cloned.1.call-update) | async-done | bytes 1310736 | tf_op jit(solution)/shard_map/reduce_scatter | solution.py:56
  328.7 2.9 add_convert_fusion.2
  331.7 0.7 convert_element_type.98
  332.5 0.7 convert_element_type.97
  334.2 21.1 %all-gather.1 = f32[8,1,256]{2,1,0:T(1,128)S(1)} all-gather(f32[1,1,256]{2,1,0:T(1,128)S(1)} %bitcast.35), channel_id=1, replica_groups=mesh['rep'=2,'fs'=8,'tp'=2] {'fs'}, dimensions={0}, use_global_device_ids=true | all-gather | bytes 9216 | tf_op jit(solution)/shard_map/all_gather | solution.py:42
  355.3 2.6 fusion.3
  357.9 38.9 %all-gather.24.cloned.1.call-done = bf16[2048,512]{1,0:T(8,128)(2,1)} async-done(((bf16[256,512]{1,0:T(8,128)(2,1)}), bf16[2048,512]{1,0:T(8,128)(2,1)}) %all-gather.24.cloned.1.call-update) | async-done | bytes 2097168 | tf_op jit(solution)/shard_map/all_gather | solution.py:84
  396.8 4.6 fusion.57
  401.4 2.6 all-reduce
  404.1 1.6 add_convert_fusion.3
  406.3 1.0 copy.26
  407.3 39.3 %all-gather.22.cloned.1.call-done = bf16[2048,512]{1,0:T(8,128)(2,1)} async-done(((bf16[256,512]{1,0:T(8,128)(2,1)}), bf16[2048,512]{1,0:T(8,128)(2,1)}) %all-gather.22.cloned.1.call-update) | async-done | bytes 2097168 | tf_op jit(solution)/shard_map/all_gather | solution.py:83
  446.6 51.0 %all-gather.26.cloned.1.call-done = bf16[512,2048]{1,0:T(8,128)(2,1)} async-done(((bf16[512,256]{1,0:T(8,128)(2,1)}), bf16[512,2048]{1,0:T(8,128)(2,1)}) %all-gather.26.cloned.1.call-update) | async-done | bytes 2097168 | tf_op jit(solution)/shard_map/all_gather | solution.py:107
  497.6 7.8 %multiply_convert_fusion.1 = bf16[640,2048]{1,0:T(8,128)(2,1)} fusion(bf16[512,2048]{1,0:T(8,128)(2,1)} %all-gather.26.cloned.1.call-done, f32[2048]{0:T(1024)S(1)} %bitcast.32, f32[80,8,4,128]{3,2,1,0:T(4,128)S(1)} %bitcast.29, bf16[2048,512]{1,0:T(8,128)(2,1)} %all-gather.22.cloned.1.call-done, bf16[640,2048]{1,0:T(8,128)(2,1)} %all-gather.20.cloned.1.call-done, ...), kind=kOutput, calls=%fused_computation.16 | convolution fusion | flops 2695823360 | bytes 10768896 | tf_op jit(solution)/shard_map/dot_general | solution.py:105
  505.4 8.6 %reduce-scatter.6.cloned.1.call-done = bf16[640,1024]{1,0:T(8,128)(2,1)} async-done(((bf16[640,2048]{1,0:T(8,128)(2,1)}), bf16[640,1024]{1,0:T(8,128)(2,1)}) %reduce-scatter.6.cloned.1.call-update) | async-done | bytes 1310736 | tf_op jit(solution)/shard_map/reduce_scatter | solution.py:56
  514.0 2.9 add_convert_fusion.1
  517.2 12.5 %all-gather.28.cloned.1.call-done = bf16[640,2048]{1,0:T(8,128)(2,1)} async-done(((bf16[640,1024]{1,0:T(8,128)(2,1)}), bf16[640,2048]{1,0:T(8,128)(2,1)}) %all-gather.28.cloned.1.call-update) | async-done | bytes 2621456 | tf_op jit(solution)/shard_map/all_gather | solution.py:50
  529.7 2.5 fusion.6
  532.2 8.7 %convolution_multiply_fusion.1 = f32[640,1408]{1,0:T(8,128)} fusion(bf16[2048,1408]{1,0:T(8,128)(2,1)} %all-gather.14.cloned.1.call-done, f32[1408]{0:T(1024)S(1)} %copy-done.19, bf16[640,2048]{1,0:T(8,128)(2,1)S(1)} %copy-done.5, f32[2048]{0:T(1024)S(1)} %copy-done.21, f32[640]{0:T(1024)S(1)} %add_rsqrt_fusion), kind=kOutput, calls=%fused_computation.20 | convolution fusion | flops 3697131520 | bytes 12009472 | tf_op jit(solution)/shard_map/dot_general | solution.py:66
  540.9 15.4 %multiply_convert_fusion = bf16[640,2048]{1,0:T(8,128)(2,1)} fusion(bf16[1408,2048]{1,0:T(8,128)(2,1)} %all-gather.18.cloned.1.call-done, f32[2048]{0:T(1024)S(1)} %bitcast.31, bf16[2048,1408]{1,0:T(8,128)(2,1)} %all-gather.16.cloned.1.call-done, f32[640,1408]{1,0:T(8,128)} %convolution_multiply_fusion.1, f32[1408]{0:T(1024)S(1)} %copy-done.20, ...), kind=kOutput, calls=%fused_computation.15 | convolution fusion | flops 7396147200 | bytes 20406272 | tf_op jit(solution)/shard_map/dot_general | solution.py:115
  556.3 11.6 %reduce-scatter.8.cloned.1.call-done = bf16[640,1024]{1,0:T(8,128)(2,1)} async-done(((bf16[640,2048]{1,0:T(8,128)(2,1)}), bf16[640,1024]{1,0:T(8,128)(2,1)}) %reduce-scatter.8.cloned.1.call-update) | async-done | bytes 1310736 | tf_op jit(solution)/shard_map/reduce_scatter | solution.py:56
  567.9 2.9 add_convert_fusion
  (82 shorter events, 3.1 us)
Async XLA Ops:
  6.5 3.3 copy-start.6
  6.5 27.7 %all-gather.12.cloned.1.call-start = ((), (), s32[]{:S(2)}) async-start(), calls=%async_computation.3 | async-start | bytes 3932160 | tf_op jit(solution)/shard_map/all_gather | solution.py:50
  7.3 3.6 copy-start.7
  7.3 111.4 %all-gather.14.cloned.1.call-start = ((), (), s32[]{:S(2)}) async-start(), calls=%async_computation.4 | async-start | bytes 6488064 | tf_op jit(solution)/shard_map/all_gather | solution.py:61
  9.8 201.6 %all-gather.16.cloned.1.call-start = ((), (), s32[]{:S(2)}) async-start(), calls=%async_computation.5 | async-start | bytes 6488064 | tf_op jit(solution)/shard_map/all_gather | solution.py:62
  10.8 107.9 %copy-start.17 = (f32[2048]{0:T(1024)S(1)}, f32[2048]{0:T(1024)}, u32[]{:S(2)}) copy-start(f32[2048]{0:T(1024)} %param.21) | copy-start | bytes 24580
  10.8 107.9 %copy-start.19 = (f32[1408]{0:T(1024)S(1)}, f32[1408]{0:T(1024)}, u32[]{:S(2)}) copy-start(f32[1408]{0:T(1024)} %param.27) | copy-start | bytes 16900
  10.8 293.8 %all-gather.18.cloned.1.call-start = ((), (), s32[]{:S(2)}) async-start(), calls=%async_computation.6 | async-start | bytes 6488064 | tf_op jit(solution)/shard_map/all_gather | solution.py:71
  11.8 316.8 %reduce-scatter.4.cloned.1.call-start = ((), (), s32[]{:S(2)}) async-start(), calls=%async_computation.7 | async-start | bytes 3932160 | tf_op jit(solution)/shard_map/reduce_scatter | solution.py:56
  34.2 84.5 %copy-start.4 = (bf16[640,2048]{1,0:T(8,128)(2,1)S(1)}, bf16[640,2048]{1,0:T(8,128)(2,1)}, u32[]{:S(2)}) copy-start(bf16[640,2048]{1,0:T(8,128)(2,1)} %all-gather.12.cloned.1.call-done) | copy-start | bytes 7864324
  36.9 267.8 %copy-start.20 = (f32[1408]{0:T(1024)S(1)}, f32[1408]{0:T(1024)}, u32[]{:S(2)}) copy-start(f32[1408]{0:T(1024)} %param.28) | copy-start | bytes 16900
  320.0 8.7 %copy-start.2 = (bf16[640,1024]{1,0:T(8,128)(2,1)S(1)}, bf16[640,1024]{1,0:T(8,128)(2,1)}, u32[]{:S(2)}) copy-start(bf16[640,1024]{1,0:T(8,128)(2,1)} %param.20) | copy-start | bytes 3932164
  320.1 11.6 %copy-start.8 = (f32[256,512]{1,0:T(8,128)S(1)}, f32[256,512]{1,0:T(8,128)}, u32[]{:S(2)}) copy-start(f32[256,512]{1,0:T(8,128)} %param.31) | copy-start | bytes 1572868
  320.1 12.5 %copy-start.9 = (f32[256,512]{1,0:T(8,128)S(1)}, f32[256,512]{1,0:T(8,128)}, u32[]{:S(2)}) copy-start(f32[256,512]{1,0:T(8,128)} %param.30) | copy-start | bytes 1572868
  320.1 35.2 %all-gather.20.cloned.1.call-start = ((), (), s32[]{:S(2)}) async-start(), calls=%async_computation.8 | async-start | bytes 3932160 | tf_op jit(solution)/shard_map/all_gather | solution.py:50
  331.6 65.2 %all-gather.24.cloned.1.call-start = ((), (), s32[]{:S(2)}) async-start(), calls=%async_computation.10 | async-start | bytes 2359296 | tf_op jit(solution)/shard_map/all_gather | solution.py:84
  332.4 64.4 %copy-start.18 = (f32[2048]{0:T(1024)S(1)}, f32[2048]{0:T(1024)}, u32[]{:S(2)}) copy-start(f32[2048]{0:T(1024)} %param.22) | copy-start | bytes 24580
  332.4 64.4 %copy-start.22 = (f32[512]{0:T(512)S(1)}, f32[512]{0:T(512)}, u32[]{:S(2)}) copy-start(f32[512]{0:T(512)} %param.33) | copy-start | bytes 6148
  332.5 114.1 %all-gather.22.cloned.1.call-start = ((), (), s32[]{:S(2)}) async-start(), calls=%async_computation.9 | async-start | bytes 2359296 | tf_op jit(solution)/shard_map/all_gather | solution.py:83
  333.3 164.3 %all-gather.26.cloned.1.call-start = ((), (), s32[]{:S(2)}) async-start(), calls=%async_computation.11 | async-start | bytes 2359296 | tf_op jit(solution)/shard_map/all_gather | solution.py:107
  334.1 179.9 %reduce-scatter.6.cloned.1.call-start = ((), (), s32[]{:S(2)}) async-start(), calls=%async_computation.12 | async-start | bytes 3932160 | tf_op jit(solution)/shard_map/reduce_scatter | solution.py:56
  355.3 41.5 %copy-start.3 = (bf16[640,2048]{1,0:T(8,128)(2,1)S(1)}, bf16[640,2048]{1,0:T(8,128)(2,1)}, u32[]{:S(2)}) copy-start(bf16[640,2048]{1,0:T(8,128)(2,1)} %all-gather.20.cloned.1.call-done) | copy-start | bytes 7864324
  357.9 46.2 %copy-start.13 = (f32[512]{0:T(512)S(1)}, f32[512]{0:T(512)}, u32[]{:S(2)}) copy-start(f32[512]{0:T(512)} %param.35) | copy-start | bytes 6148
  357.9 46.2 %copy-start.14 = (f32[512]{0:T(512)S(1)}, f32[512]{0:T(512)}, u32[]{:S(2)}) copy-start(f32[512]{0:T(512)} %param.34) | copy-start | bytes 6148
  401.4 4.4 copy-start.11
  401.4 4.5 copy-start.12
  405.9 91.7 %copy-start.23 = (f32[512]{0:T(512)S(1)}, f32[512]{0:T(512)}, u32[]{:S(2)}) copy-start(f32[512]{0:T(512)} %param.32) | copy-start | bytes 6148
  505.3 8.7 %copy-start = (bf16[640,1024]{1,0:T(8,128)(2,1)S(1)}, bf16[640,1024]{1,0:T(8,128)(2,1)}, u32[]{:S(2)}) copy-start(bf16[640,1024]{1,0:T(8,128)(2,1)} %add_convert_fusion.2) | copy-start | bytes 3932164
  505.4 24.4 %all-gather.28.cloned.1.call-start = ((), (), s32[]{:S(2)}) async-start(), calls=%async_computation.13 | async-start | bytes 3932160 | tf_op jit(solution)/shard_map/all_gather | solution.py:50
  516.9 15.3 %copy-start.21 = (f32[2048]{0:T(1024)S(1)}, f32[2048]{0:T(1024)}, u32[]{:S(2)}) copy-start(f32[2048]{0:T(1024)} %param.23) | copy-start | bytes 24580
  516.9 51.0 %reduce-scatter.8.cloned.1.call-start = ((), (), s32[]{:S(2)}) async-start(), calls=%async_computation.14 | async-start | bytes 3932160 | tf_op jit(solution)/shard_map/reduce_scatter | solution.py:56
  556.3 11.6 %copy-start.1 = (bf16[640,1024]{1,0:T(8,128)(2,1)S(1)}, bf16[640,1024]{1,0:T(8,128)(2,1)}, u32[]{:S(2)}) copy-start(bf16[640,1024]{1,0:T(8,128)(2,1)} %add_convert_fusion.1) | copy-start | bytes 3932164
  (4 other events, 8.9 us)
Sparse Core Ops, SparseCore 0:
  8.9 14.0 all-gather.11
  25.2 93.4 all-gather.13
  120.9 90.4 all-gather.15
  213.3 91.2 all-gather.17
  320.2 8.4 reduce-scatter.3
  331.8 12.6 all-gather.19
  346.5 50.2 all-gather.23
  399.0 47.6 all-gather.21
  448.7 48.8 all-gather.25
  505.5 8.4 reduce-scatter.5
  517.0 12.6 all-gather.27
  556.4 11.4 reduce-scatter.7
where the time goes:
time: 578 us
  waiting for transfers between devices  430 us (74%)
  matrix products  60.8 us (11%)
  blocking collectives  46 us (8%)
  other arithmetic  24.6 us (4%)
  between operations  13.8 us (2%)
    all_gather x1, waiting for transfers between devices, on_device(): down_all = lax.all_gather(down_low, 'fs', axis=1, tiled=True)  93.2 us
    all_gather x1, waiting for transfers between devices, on_device(): lax.all_gather(up_low, 'fs', axis=0, tiled=True)  84 us
    all_gather x1, waiting for transfers between devices, on_device(): lax.all_gather(gate_low, 'fs', axis=0, tiled=True)  81.8 us
    all_gather x1, waiting for transfers between devices, on_device(): lax.all_gather(out_low, 'fs', axis=1, tiled=True)  51 us
    all_gather x1, waiting for transfers between devices, on_device(): lax.all_gather(u_low, 'fs', axis=0, tiled=True)  39.3 us
    all_gather x1, waiting for transfers between devices, on_device(): lax.all_gather(v_low, 'fs', axis=0, tiled=True)  38.9 us
    reduce_scatter x3, waiting for transfers between devices, spread_sum(): lax.psum_scatter(term.astype(jnp.bfloat16), 'tp', scatter_dimension=1, ti...  28.7 us
    all_gather x1, blocking collectives, on_device(): lax.all_gather(down_scale, 'fs', axis=0, tiled=True)  22.3 us
  transfers between devices with their start and end apart: 12, of which 10 were waited for; matrix products, arithmetic and copies ran while one was open for 5% of the time, Pallas kernels for 0%

commit v1 on v0

--- a/solution.py
+++ b/solution.py
@@ -68,7 +68,12 @@
         return (jax.nn.silu(gate) * up_part).astype(jnp.bfloat16)
 
     first_hidden = hidden_units(full_norm(tokens, norm_first))
-    down_all = lax.all_gather(down_low, "fs", axis=1, tiled=True)
+    ring = [down_low]
+    for hop in range(7):
+        ring.append(lax.ppermute(ring[-1], "fs", [(dev, (dev + 1) % 8) for dev in range(8)]))
+    down_all = jnp.roll(
+        jnp.concatenate(ring[::-1], axis=1), (lax.axis_index("fs") + 1) * ring[0].shape[1], axis=1
+    )
     first_term = (
         jnp.dot(first_hidden, down_all, preferred_element_type=jnp.float32) * wide_scales[0]
     )

time: 578 us -> 555 us (0.960)
  waiting for transfers between devices: 430 us -> 358 us
  blocking collectives: 46 us -> 68.3 us
  local copies, waits for them, and re-layouts: 1.29 us -> 21.9 us
    ppermute x0 -> x7, waiting for transfers between devices: none -> 166 us  [on_device(): lax.ppermute(ring[-1], 'fs', [(dev, (dev + 1) % 8) for dev in range(8)])]
    all_gather x1 -> x0, waiting for transfers between devices: 93.2 us -> none  [on_device(): down_all = lax.all_gather(down_low, 'fs', axis=1, tiled=True)]
    all_gather x1, waiting for transfers between devices: 81.8 us -> 0.01 us  [on_device(): lax.all_gather(gate_low, 'fs', axis=0, tiled=True)]
    all_gather x1, waiting for transfers between devices: 84 us -> 18.7 us  [on_device(): lax.all_gather(up_low, 'fs', axis=0, tiled=True)]
    all_gather x1, blocking collectives: 22.3 us -> 44.9 us  [on_device(): lax.all_gather(down_scale, 'fs', axis=0, tiled=True)]
    unnamed x48 -> x66, local copies, waits for them, and re-layouts: 0.15 us -> 20.8 us
  transfers between devices with their start and end apart: 12 -> 18, of which waited for: 10 -> 14; matrix products, arithmetic and copies ran while one was open for 5% -> 9% of each run, Pallas kernels for 0% -> 0%
where the time goes in v1:
time: 555 us; the launch traced here: 554 us
  waiting for transfers between devices  358 us (65%)
  blocking collectives  68.3 us (12%)
  matrix products  64.2 us (12%)
  other arithmetic  25.2 us (5%)
  local copies, waits for them, and re-layouts  21.9 us (4%)
  between operations  13.5 us (2%)
    ppermute x7, waiting for transfers between devices, on_device(): lax.ppermute(ring[-1], 'fs', [(dev, (dev + 1) % 8) for dev in range(8)])  166 us
    all_gather x1, waiting for transfers between devices, on_device(): lax.all_gather(out_low, 'fs', axis=1, tiled=True)  51 us
    all_gather x1, blocking collectives, on_device(): lax.all_gather(down_scale, 'fs', axis=0, tiled=True)  44.9 us
    all_gather x1, waiting for transfers between devices, on_device(): lax.all_gather(u_low, 'fs', axis=0, tiled=True)  41 us
    all_gather x1, waiting for transfers between devices, on_device(): lax.all_gather(v_low, 'fs', axis=0, tiled=True)  39.1 us
    reduce_scatter x3, waiting for transfers between devices, spread_sum(): lax.psum_scatter(term.astype(jnp.bfloat16), 'tp', scatter_dimension=1, ti...  28.6 us
    all_gather x1, blocking collectives, on_device(): lax.all_gather(out_scale, 'fs', axis=0, tiled=True)  20.9 us
    unnamed x66, local copies, waits for them, and re-layouts  20.8 us
  transfers between devices with their start and end apart: 18, of which 14 were waited for; matrix products, arithmetic and copies ran while one was open for 9% of the time, Pallas kernels for 0%

profile of v1, /device:TPU:0, one launch (start us, length us, event | category | flops | bytes accessed | tf_op | source)
XLA Modules:
  0.0 554.4 jit_solution(9326004618954592566)
XLA Ops:
  7.3 2.3 convert_element_type.87
  9.8 3.0 collective-permute-start
  12.8 2.3 convert_element_type.88
  15.2 16.8 %collective-permute-done = bf16[1408,256]{1,0:T(8,128)(2,1)S(1)} collective-permute-done((bf16[1408,256]{1,0:T(8,128)(2,1)S(1)}, bf16[1408,256]{1,0:T(8,128)(2,1)S(1)}, u32[]{:S(2)}, u32[]{:S(2)}) %collective-permute-start) | collective-permute-done | bytes 720928 | tf_op jit(solution)/shard_map/ppermute | solution.py:73
  32.0 33.4 %collective-permute-done.1 = bf16[1408,256]{1,0:T(8,128)(2,1)S(1)} collective-permute-done((bf16[1408,256]{1,0:T(8,128)(2,1)S(1)}, bf16[1408,256]{1,0:T(8,128)(2,1)S(1)}, u32[]{:S(2)}, u32[]{:S(2)}) %collective-permute-start.1) | collective-permute-done | bytes 720928 | tf_op jit(solution)/shard_map/ppermute | solution.py:73
  65.4 25.3 %collective-permute-done.2 = bf16[1408,256]{1,0:T(8,128)(2,1)S(1)} collective-permute-done((bf16[1408,256]{1,0:T(8,128)(2,1)S(1)}, bf16[1408,256]{1,0:T(8,128)(2,1)S(1)}, u32[]{:S(2)}, u32[]{:S(2)}) %collective-permute-start.2) | collective-permute-done | bytes 720928 | tf_op jit(solution)/shard_map/ppermute | solution.py:73
  91.6 36.3 %collective-permute-done.3 = bf16[1408,256]{1,0:T(8,128)(2,1)S(1)} collective-permute-done((bf16[1408,256]{1,0:T(8,128)(2,1)S(1)}, bf16[1408,256]{1,0:T(8,128)(2,1)S(1)}, u32[]{:S(2)}, u32[]{:S(2)}) %collective-permute-start.3) | collective-permute-done | bytes 720928 | tf_op jit(solution)/shard_map/ppermute | solution.py:73
  128.7 36.0 %collective-permute-done.4 = bf16[1408,256]{1,0:T(8,128)(2,1)S(1)} collective-permute-done((bf16[1408,256]{1,0:T(8,128)(2,1)S(1)}, bf16[1408,256]{1,0:T(8,128)(2,1)S(1)}, u32[]{:S(2)}, u32[]{:S(2)}) %collective-permute-start.4) | collective-permute-done | bytes 720928 | tf_op jit(solution)/shard_map/ppermute | solution.py:73
  165.6 18.1 %collective-permute-done.5 = bf16[1408,256]{1,0:T(8,128)(2,1)} collective-permute-done((bf16[1408,256]{1,0:T(8,128)(2,1)S(1)}, bf16[1408,256]{1,0:T(8,128)(2,1)}, u32[]{:S(2)}, u32[]{:S(2)}) %collective-permute-start.5) | collective-permute-done | bytes 720928 | tf_op jit(solution)/shard_map/ppermute | solution.py:73
  183.7 44.9 %all-gather = f32[8,1,256]{2,1,0:T(1,128)S(1)} all-gather(f32[1,1,256]{2,1,0:T(1,128)S(1)} %bitcast.32), channel_id=1, replica_groups=mesh['rep'=2,'fs'=8,'tp'=2] {'fs'}, dimensions={0}, use_global_device_ids=true | all-gather | bytes 9216 | tf_op jit(solution)/shard_map/all_gather | solution.py:41
  228.6 2.5 fusion
  251.2 9.6 %convolution_multiply_fusion.3 = f32[640,1408]{1,0:T(8,128)} fusion(bf16[2048,1408]{1,0:T(8,128)(2,1)} %all-gather.13.cloned.1.call-done, f32[1408]{0:T(1024)S(1)} %copy-done.21, bf16[640,2048]{1,0:T(8,128)(2,1)} %all-gather.11.cloned.1.call-done, f32[2048]{0:T(1024)S(1)} %copy-done.19, f32[640]{0:T(1024)S(1)} %add_rsqrt_fusion.3), kind=kOutput, calls=%fused_computation.27 | convolution fusion | flops 3697131520 | bytes 12009472 | tf_op jit(solution)/shard_map/dot_general | solution.py:66
  260.8 18.7 %all-gather.15.cloned.1.call-done = bf16[2048,1408]{1,0:T(8,128)(2,1)} async-done(((bf16[256,1408]{1,0:T(8,128)(2,1)}), bf16[2048,1408]{1,0:T(8,128)(2,1)}) %all-gather.15.cloned.1.call-update) | async-done | bytes 5767184 | tf_op jit(solution)/shard_map/all_gather | solution.py:62
  279.5 16.2 %multiply_convert_fusion.2 = bf16[640,2048]{1,0:T(8,128)(2,1)} fusion(bf16[1408,4096]{1,0:T(8,128)(2,1)} %constant_dynamic-update-slice_fusion, s32[]{:T(128)S(6)} %select_n.20, f32[2048]{0:T(1024)S(1)} %bitcast.28, bf16[2048,1408]{1,0:T(8,128)(2,1)} %all-gather.15.cloned.1.call-done, f32[640,1408]{1,0:T(8,128)} %convolution_multiply_fusion.3, ...), kind=kOutput, calls=%fused_computation.17 | convolution fusion | flops 7396147200 | bytes 20406276 | tf_op jit(solution)/shard_map/dot_general | solution.py:78
  295.9 8.4 %reduce-scatter.4.cloned.1.call-done = bf16[640,1024]{1,0:T(8,128)(2,1)} async-done(((bf16[640,2048]{1,0:T(8,128)(2,1)}), bf16[640,1024]{1,0:T(8,128)(2,1)}) %reduce-scatter.4.cloned.1.call-update) | async-done | bytes 1310736 | tf_op jit(solution)/shard_map/reduce_scatter | solution.py:56
  304.3 2.9 add_convert_fusion.2
  309.7 20.9 %all-gather.1 = f32[8,1,256]{2,1,0:T(1,128)S(1)} all-gather(f32[1,1,256]{2,1,0:T(1,128)S(1)} %bitcast.33), channel_id=1, replica_groups=mesh['rep'=2,'fs'=8,'tp'=2] {'fs'}, dimensions={0}, use_global_device_ids=true | all-gather | bytes 9216 | tf_op jit(solution)/shard_map/all_gather | solution.py:42
  330.7 2.4 fusion.3
  333.2 39.1 %all-gather.21.cloned.1.call-done = bf16[2048,512]{1,0:T(8,128)(2,1)} async-done(((bf16[256,512]{1,0:T(8,128)(2,1)}), bf16[2048,512]{1,0:T(8,128)(2,1)}) %all-gather.21.cloned.1.call-update) | async-done | bytes 2097168 | tf_op jit(solution)/shard_map/all_gather | solution.py:89
  372.3 4.4 fusion.67
  376.7 2.5 all-reduce
  381.1 41.0 %all-gather.19.cloned.1.call-done = bf16[2048,512]{1,0:T(8,128)(2,1)} async-done(((bf16[256,512]{1,0:T(8,128)(2,1)}), bf16[2048,512]{1,0:T(8,128)(2,1)}) %all-gather.19.cloned.1.call-update) | async-done | bytes 2097168 | tf_op jit(solution)/shard_map/all_gather | solution.py:88
  422.1 51.0 %all-gather.23.cloned.1.call-done = bf16[512,2048]{1,0:T(8,128)(2,1)} async-done(((bf16[512,256]{1,0:T(8,128)(2,1)}), bf16[512,2048]{1,0:T(8,128)(2,1)}) %all-gather.23.cloned.1.call-update) | async-done | bytes 2097168 | tf_op jit(solution)/shard_map/all_gather | solution.py:112
  473.0 7.8 %multiply_convert_fusion.1 = bf16[640,2048]{1,0:T(8,128)(2,1)} fusion(bf16[512,2048]{1,0:T(8,128)(2,1)} %all-gather.23.cloned.1.call-done, f32[2048]{0:T(1024)S(1)} %bitcast.30, f32[80,8,4,128]{3,2,1,0:T(4,128)S(1)} %bitcast.27, bf16[2048,512]{1,0:T(8,128)(2,1)} %all-gather.19.cloned.1.call-done, bf16[640,2048]{1,0:T(8,128)(2,1)} %all-gather.17.cloned.1.call-done, ...), kind=kOutput, calls=%fused_computation.16 | convolution fusion | flops 2695823360 | bytes 10768896 | tf_op jit(solution)/shard_map/dot_general | solution.py:110
  480.9 8.6 %reduce-scatter.6.cloned.1.call-done = bf16[640,1024]{1,0:T(8,128)(2,1)} async-done(((bf16[640,2048]{1,0:T(8,128)(2,1)}), bf16[640,1024]{1,0:T(8,128)(2,1)}) %reduce-scatter.6.cloned.1.call-update) | async-done | bytes 1310736 | tf_op jit(solution)/shard_map/reduce_scatter | solution.py:56
  489.5 2.9 add_convert_fusion.1
  492.7 12.5 %all-gather.25.cloned.1.call-done = bf16[640,2048]{1,0:T(8,128)(2,1)} async-done(((bf16[640,1024]{1,0:T(8,128)(2,1)}), bf16[640,2048]{1,0:T(8,128)(2,1)}) %all-gather.25.cloned.1.call-update) | async-done | bytes 2621456 | tf_op jit(solution)/shard_map/all_gather | solution.py:50
  505.2 2.3 fusion.6
  507.6 9.5 %convolution_multiply_fusion.1 = f32[640,1408]{1,0:T(8,128)} fusion(bf16[2048,1408]{1,0:T(8,128)(2,1)} %all-gather.13.cloned.1.call-done, f32[1408]{0:T(1024)S(1)} %copy-done.21, bf16[640,2048]{1,0:T(8,128)(2,1)} %all-gather.25.cloned.1.call-done, f32[2048]{0:T(1024)S(1)} %copy-done.23, f32[640]{0:T(1024)S(1)} %add_rsqrt_fusion), kind=kOutput, calls=%fused_computation.24 | convolution fusion | flops 3697131520 | bytes 12009472 | tf_op jit(solution)/shard_map/dot_general | solution.py:66
  517.1 16.2 %multiply_convert_fusion = bf16[640,2048]{1,0:T(8,128)(2,1)} fusion(bf16[1408,4096]{1,0:T(8,128)(2,1)} %constant_dynamic-update-slice_fusion, s32[]{:T(128)S(6)} %select_n.20, f32[2048]{0:T(1024)S(1)} %bitcast.29, bf16[2048,1408]{1,0:T(8,128)(2,1)} %all-gather.15.cloned.1.call-done, f32[640,1408]{1,0:T(8,128)} %convolution_multiply_fusion.1, ...), kind=kOutput, calls=%fused_computation.15 | convolution fusion | flops 7396147200 | bytes 20406276 | tf_op jit(solution)/shard_map/dot_general | solution.py:120
  533.3 11.6 %reduce-scatter.8.cloned.1.call-done = bf16[640,1024]{1,0:T(8,128)(2,1)} async-done(((bf16[640,2048]{1,0:T(8,128)(2,1)}), bf16[640,1024]{1,0:T(8,128)(2,1)}) %reduce-scatter.8.cloned.1.call-update) | async-done | bytes 1310736 | tf_op jit(solution)/shard_map/reduce_scatter | solution.py:56
  545.0 2.9 add_convert_fusion
  (113 shorter events, 28.6 us)
Async XLA Ops:
  6.5 222.1 %all-gather.11.cloned.1.call-start = ((), (), s32[]{:S(2)}) async-start(), calls=%async_computation.3 | async-start | bytes 3932160 | tf_op jit(solution)/shard_map/all_gather | solution.py:50
  7.3 176.5 %copy-start.17 = (f32[256]{0:T(256)S(1)}, f32[256]{0:T(256)}, u32[]{:S(2)}) copy-start(f32[256]{0:T(256)} %param.29) | copy-start | bytes 3076
  7.3 243.9 %all-gather.13.cloned.1.call-start = ((), (), s32[]{:S(2)}) async-start(), calls=%async_computation.4 | async-start | bytes 6488064 | tf_op jit(solution)/shard_map/all_gather | solution.py:61
  9.6 269.8 %all-gather.15.cloned.1.call-start = ((), (), s32[]{:S(2)}) async-start(), calls=%async_computation.5 | async-start | bytes 6488064 | tf_op jit(solution)/shard_map/all_gather | solution.py:62
  9.8 22.2 %collective-permute-start = (bf16[1408,256]{1,0:T(8,128)(2,1)S(1)}, bf16[1408,256]{1,0:T(8,128)(2,1)S(1)}, u32[]{:S(2)}, u32[]{:S(2)}) collective-permute-start(bf16[1408,256]{1,0:T(8,128)(2,1)S(1)} %convert_element_type.90), channel_id=1, source_target_pairs={{0,2},{2,4},{4,6},{6,8},{8,10},{10,12},{12,14},{14,0},{1,3},{3,5},... | collective-permute-start | bytes 2162696 | tf_op jit(solution)/shard_map/ppermute | solution.py:73
  15.2 289.1 %reduce-scatter.4.cloned.1.call-start = ((), (), s32[]{:S(2)}) async-start(), calls=%async_computation.6 | async-start | bytes 3932160 | tf_op jit(solution)/shard_map/reduce_scatter | solution.py:56
  32.0 33.4 %collective-permute-start.1 = (bf16[1408,256]{1,0:T(8,128)(2,1)S(1)}, bf16[1408,256]{1,0:T(8,128)(2,1)S(1)}, u32[]{:S(2)}, u32[]{:S(2)}) collective-permute-start(bf16[1408,256]{1,0:T(8,128)(2,1)S(1)} %collective-permute-done), channel_id=1, source_target_pairs={{0,2},{2,4},{4,6},{6,8},{8,10},{10,12},{12,14},{14,0},{1,3},{3,5},... | collective-permute-start | bytes 2162696 | tf_op jit(solution)/shard_map/ppermute | solution.py:73
  65.4 25.3 %collective-permute-start.2 = (bf16[1408,256]{1,0:T(8,128)(2,1)S(1)}, bf16[1408,256]{1,0:T(8,128)(2,1)S(1)}, u32[]{:S(2)}, u32[]{:S(2)}) collective-permute-start(bf16[1408,256]{1,0:T(8,128)(2,1)S(1)} %collective-permute-done.1), channel_id=1, source_target_pairs={{0,2},{2,4},{4,6},{6,8},{8,10},{10,12},{12,14},{14,0},{1,3},{3,5},... | collective-permute-start | bytes 2162696 | tf_op jit(solution)/shard_map/ppermute | solution.py:73
  91.6 36.3 %collective-permute-start.3 = (bf16[1408,256]{1,0:T(8,128)(2,1)S(1)}, bf16[1408,256]{1,0:T(8,128)(2,1)S(1)}, u32[]{:S(2)}, u32[]{:S(2)}) collective-permute-start(bf16[1408,256]{1,0:T(8,128)(2,1)S(1)} %collective-permute-done.2), channel_id=1, source_target_pairs={{0,2},{2,4},{4,6},{6,8},{8,10},{10,12},{12,14},{14,0},{1,3},{3,5},... | collective-permute-start | bytes 2162696 | tf_op jit(solution)/shard_map/ppermute | solution.py:73
  128.7 36.0 %collective-permute-start.4 = (bf16[1408,256]{1,0:T(8,128)(2,1)S(1)}, bf16[1408,256]{1,0:T(8,128)(2,1)S(1)}, u32[]{:S(2)}, u32[]{:S(2)}) collective-permute-start(bf16[1408,256]{1,0:T(8,128)(2,1)S(1)} %collective-permute-done.3), channel_id=1, source_target_pairs={{0,2},{2,4},{4,6},{6,8},{8,10},{10,12},{12,14},{14,0},{1,3},{3,5},... | collective-permute-start | bytes 2162696 | tf_op jit(solution)/shard_map/ppermute | solution.py:73
  165.6 18.1 %collective-permute-start.5 = (bf16[1408,256]{1,0:T(8,128)(2,1)S(1)}, bf16[1408,256]{1,0:T(8,128)(2,1)}, u32[]{:S(2)}, u32[]{:S(2)}) collective-permute-start(bf16[1408,256]{1,0:T(8,128)(2,1)S(1)} %collective-permute-done.4), channel_id=1, source_target_pairs={{0,2},{2,4},{4,6},{6,8},{8,10},{10,12},{12,14},{14,0},{1,3},{3,5},... | collective-permute-start | bytes 2162696 | tf_op jit(solution)/shard_map/ppermute | solution.py:73
  183.7 47.4 %collective-permute-start.6 = (bf16[1408,256]{1,0:T(8,128)(2,1)}, bf16[1408,256]{1,0:T(8,128)(2,1)}, u32[]{:S(2)}, u32[]{:S(2)}) collective-permute-start(bf16[1408,256]{1,0:T(8,128)(2,1)} %collective-permute-done.5), channel_id=1, source_target_pairs={{0,2},{2,4},{4,6},{6,8},{8,10},{10,12},{12,14},{14,0},{1,3},{3,5},... | collective-permute-start | bytes 2162696 | tf_op jit(solution)/shard_map/ppermute | solution.py:73
  251.2 28.3 %copy-start.22 = (f32[1408]{0:T(1024)S(1)}, f32[1408]{0:T(1024)}, u32[]{:S(2)}) copy-start(f32[1408]{0:T(1024)} %param.28) | copy-start | bytes 16900
  279.4 24.8 %copy-start.3 = (bf16[640,1024]{1,0:T(8,128)(2,1)S(1)}, bf16[640,1024]{1,0:T(8,128)(2,1)}, u32[]{:S(2)}) copy-start(bf16[640,1024]{1,0:T(8,128)(2,1)} %param.20) | copy-start | bytes 3932164
  295.7 14.1 %copy-start.18 = (f32[256]{0:T(256)S(1)}, f32[256]{0:T(256)}, u32[]{:S(2)}) copy-start(f32[256]{0:T(256)} %param.39) | copy-start | bytes 3076
  295.7 35.0 %all-gather.17.cloned.1.call-start = ((), (), s32[]{:S(2)}) async-start(), calls=%async_computation.7 | async-start | bytes 3932160 | tf_op jit(solution)/shard_map/all_gather | solution.py:50
  307.2 65.1 %copy-start.20 = (f32[2048]{0:T(1024)S(1)}, f32[2048]{0:T(1024)}, u32[]{:S(2)}) copy-start(f32[2048]{0:T(1024)} %param.22) | copy-start | bytes 24580
  307.2 65.1 %copy-start.24 = (f32[512]{0:T(512)S(1)}, f32[512]{0:T(512)}, u32[]{:S(2)}) copy-start(f32[512]{0:T(512)} %param.33) | copy-start | bytes 6148
  307.2 65.1 %all-gather.21.cloned.1.call-start = ((), (), s32[]{:S(2)}) async-start(), calls=%async_computation.9 | async-start | bytes 2359296 | tf_op jit(solution)/shard_map/all_gather | solution.py:89
  308.1 114.0 %all-gather.19.cloned.1.call-start = ((), (), s32[]{:S(2)}) async-start(), calls=%async_computation.8 | async-start | bytes 2359296 | tf_op jit(solution)/shard_map/all_gather | solution.py:88
  308.9 164.1 %all-gather.23.cloned.1.call-start = ((), (), s32[]{:S(2)}) async-start(), calls=%async_computation.10 | async-start | bytes 2359296 | tf_op jit(solution)/shard_map/all_gather | solution.py:112
  309.7 179.8 %reduce-scatter.6.cloned.1.call-start = ((), (), s32[]{:S(2)}) async-start(), calls=%async_computation.11 | async-start | bytes 3932160 | tf_op jit(solution)/shard_map/reduce_scatter | solution.py:56
  333.1 46.1 %copy-start.15 = (f32[512]{0:T(512)S(1)}, f32[512]{0:T(512)}, u32[]{:S(2)}) copy-start(f32[512]{0:T(512)} %param.35) | copy-start | bytes 6148
  333.1 46.1 %copy-start.16 = (f32[512]{0:T(512)S(1)}, f32[512]{0:T(512)}, u32[]{:S(2)}) copy-start(f32[512]{0:T(512)} %param.34) | copy-start | bytes 6148
  333.1 46.6 %copy-start.13 = (bf16[4,128,128]{2,1,0:T(8,128)(2,1)S(1)}, bf16[4,128,128]{2,1,0:T(8,128)(2,1)}, u32[]{:S(2)}) copy-start(bf16[4,128,128]{2,1,0:T(8,128)(2,1)} %param.36) | copy-start | bytes 393220
  333.1 46.6 %copy-start.14 = (f32[4,128]{1,0:T(4,128)S(1)}, f32[4,128]{1,0:T(4,128)}, u32[]{:S(2)}) copy-start(f32[4,128]{1,0:T(4,128)} %param.37) | copy-start | bytes 6148
  379.2 93.8 %copy-start.25 = (f32[512]{0:T(512)S(1)}, f32[512]{0:T(512)}, u32[]{:S(2)}) copy-start(f32[512]{0:T(512)} %param.32) | copy-start | bytes 6148
  473.0 16.5 %copy-start.1 = (bf16[640,1024]{1,0:T(8,128)(2,1)S(1)}, bf16[640,1024]{1,0:T(8,128)(2,1)}, u32[]{:S(2)}) copy-start(bf16[640,1024]{1,0:T(8,128)(2,1)} %add_convert_fusion.2) | copy-start | bytes 3932164
  480.9 26.7 %copy-start.23 = (f32[2048]{0:T(1024)S(1)}, f32[2048]{0:T(1024)}, u32[]{:S(2)}) copy-start(f32[2048]{0:T(1024)} %param.23) | copy-start | bytes 24580
  480.9 24.3 %all-gather.25.cloned.1.call-start = ((), (), s32[]{:S(2)}) async-start(), calls=%async_computation.12 | async-start | bytes 3932160 | tf_op jit(solution)/shard_map/all_gather | solution.py:50
  492.4 52.6 %reduce-scatter.8.cloned.1.call-start = ((), (), s32[]{:S(2)}) async-start(), calls=%async_computation.13 | async-start | bytes 3932160 | tf_op jit(solution)/shard_map/reduce_scatter | solution.py:56
  517.1 27.9 %copy-start.2 = (bf16[640,1024]{1,0:T(8,128)(2,1)S(1)}, bf16[640,1024]{1,0:T(8,128)(2,1)}, u32[]{:S(2)}) copy-start(bf16[640,1024]{1,0:T(8,128)(2,1)} %add_convert_fusion.1) | copy-start | bytes 3932164
  (12 other events, 73.9 us)
Sparse Core Ops, SparseCore 0:
  8.9 14.0 all-gather.10
  25.2 133.6 all-gather.12
  161.0 118.3 all-gather.14
  295.8 8.4 reduce-scatter.3
  307.3 12.6 all-gather.16
  322.0 50.2 all-gather.20
  374.4 47.6 all-gather.18
  424.1 48.8 all-gather.22
  481.0 8.4 reduce-scatter.5
  492.6 12.6 all-gather.24
  533.5 11.4 reduce-scatter.7
